TPU v7x, 32 devices: a whole 2x2x4 slice. The times are simulated.
32 devices in a mesh: grp: 2 (over y), kv: 4 (over z), tp: 4 (over x, core).
Axes of the slice: x: 2, y: 2, z: 4, core: 2. Of those that a mesh axis runs over, the one named last changes fastest.
Arguments:
- tokens: bfloat16 [16, 4, 2048], P('grp', None, 'kv'), parts along dimension 0, may hold values from -6 to 6
- prev_len: int32 [16], P('grp'), parts along dimension 0, may hold values from 1 to 1016, as said below
- accepted: int32 [16], P('grp'), parts along dimension 0, may hold values from 1 to 4, as said below
- parents: int32 [16, 4], P('grp'), parts along dimension 0, may hold values from -1 to 2, as said below
- cache_latent: bfloat16 [16, 1024, 256], P('grp', 'kv'), parts along dimension 0, may hold values from -210 to 210
- cache_rope: bfloat16 [16, 1024, 64], P('grp', 'kv'), parts along dimension 0, may hold values from -6 to 6
- g_pre: bfloat16 [2048], P('kv'), may hold values from 0.099609375 to 1.8984375
- w_down_q: bfloat16 [2048, 512], P('kv'), may hold values from -0.125 to 0.125
- w_down_kv: bfloat16 [2048, 256], P('kv'), may hold values from -0.125 to 0.125
- w_key_rope: bfloat16 [2048, 64], P('kv'), may hold values from -0.125 to 0.125
- g_q: bfloat16 [512], replicated, may hold values from 0.099609375 to 1.8984375
- w_up_q: bfloat16 [512, 16, 128], P(None, 'tp'), may hold values from -0.25 to 0.25
- w_q_rope: bfloat16 [512, 16, 64], P(None, 'tp'), may hold values from -0.25 to 0.25
- w_up_key: bfloat16 [256, 16, 128], P(None, 'tp'), may hold values from -0.375 to 0.375
- w_up_value: bfloat16 [256, 16, 128], P(None, 'tp'), may hold values from -0.375 to 0.375
- w_out: bfloat16 [2048, 2048], P('tp', 'kv'), may hold values from -0.125 to 0.125
- g_out: bfloat16 [2048], P('kv'), may hold values from 0.099609375 to 1.8984375
Outputs:
- mixed: bfloat16 [16, 4, 2048], P('grp', None, 'kv'), parts along dimension 0
- new_latent: bfloat16 [16, 1024, 256], P('grp', 'kv'), parts along dimension 0
- new_rope: bfloat16 [16, 1024, 64], P('grp', 'kv'), parts along dimension 0
There are 2 independent parts, one for each index of `grp`. A program takes and returns all parts, laid end to end along the dimension named above; an argument that names none is the same for every part. Nothing has to cross between parts.
Inputs may be any that keep to these rules, and one draw needn't show every extreme that they name: `prev_len`: the largest length is reached by some sequence in every draw. `accepted`: the largest count is reached by some sequence in every draw. `parents`: each parent is -1 or an earlier proposal of the same sequence; the first proposal's parent is -1.
All inputs are finite; a program needn't handle non-finite values.
Results may differ from a plain program's by a relative error of at most 0.015.
The roundings to bfloat16 on the way count: a program that leaves them out, or rounds other values in their place, can miss the bound.
Values may be sent and summed in bfloat16 or wider, within the bound.
A program may use at most 64 MiB of HBM per device.

v0:
```python
import jax
import jax.numpy as jnp
from jax import lax
from jax.sharding import PartitionSpec as P

D = 2048


EPS = 1e-06
ROPE_BASE = 10000.0
NEG_INF = -1e30


def merged(part, axis, combine):
    gathered = jax.tree.map(lambda a: lax.all_gather(a, axis), part)

    def take(source):
        return jax.tree.map(lambda a: lax.dynamic_index_in_dim(a, source, 0, False), gathered)

    return lax.fori_loop(
        1, lax.axis_size(axis), lambda source, state: combine(state, take(source)), take(0)
    )


def normalize(vector, gain):
    return (
        vector
        * lax.rsqrt(jnp.mean(vector * vector, axis=-1, keepdims=True) + EPS)
        * gain.astype(jnp.float32)
    )


def plain_normalize(vector):
    return vector * lax.rsqrt(jnp.mean(vector * vector, axis=-1, keepdims=True) + EPS)


def rotate(vector, position):
    half_dim = vector.shape[-1] // 2
    frequency = ROPE_BASE ** (-jnp.arange(half_dim, dtype=jnp.float32) / half_dim)
    angles = position.astype(jnp.float32)[..., None] * frequency
    cosine = jnp.cos(angles)
    sine_part = jnp.sin(angles)
    front = vector[..., :half_dim]
    back_part = vector[..., half_dim:]
    return jnp.concatenate(
        [front * cosine - back_part * sine_part, back_part * cosine + front * sine_part], axis=-1
    )


def ancestry(parents):
    seq_count, prop_count = parents.shape
    link = (parents[:, :, None] == jnp.arange(prop_count, dtype=jnp.int32)[None, None, :]).astype(
        jnp.float32
    )
    identity = jnp.eye(prop_count, dtype=jnp.float32)
    family = jnp.broadcast_to(identity, (seq_count, prop_count, prop_count))
    for repeat in range(prop_count):
        family = identity + jnp.einsum("sjk,skm->sjm", link, family)
    return family


def blend(earlier, later):
    peak_one, mass_one, sum_one = earlier
    peak_two, mass_two, sum_two = later
    top_all = jnp.maximum(peak_one, peak_two)
    scale_one = jnp.exp(peak_one - top_all)
    scale_two = jnp.exp(peak_two - top_all)
    return (
        top_all,
        mass_one * scale_one + mass_two * scale_two,
        sum_one * scale_one[..., None] + sum_two * scale_two[..., None],
    )


def local(
    tokens,
    prev_len,
    accepted,
    parents,
    cache_latent,
    cache_rope,
    g_pre,
    w_down_q,
    w_down_kv,
    w_key_rope,
    g_q,
    w_up_q,
    w_q_rope,
    w_up_key,
    w_up_value,
    w_out,
    g_out,
):
    f32 = jnp.float32
    bf16 = jnp.bfloat16
    seq_count, prop_count, local_dim = tokens.shape
    token_count = seq_count * prop_count
    rank_q, head_count, nope_dim = w_up_q.shape
    rope_dim = w_q_rope.shape[2]
    rank_kv = w_up_key.shape[0]
    value_dim = w_up_value.shape[2]
    span_len = cache_latent.shape[1]
    inv_root = (nope_dim + rope_dim) ** (-0.5)
    token_rows = tokens.reshape(token_count, local_dim).astype(f32)
    scaled = (token_rows * g_pre.astype(f32)).astype(bf16)
    part_q = jnp.dot(scaled, w_down_q, preferred_element_type=f32)
    part_kv = jnp.dot(scaled, w_down_kv, preferred_element_type=f32)
    part_rope = jnp.dot(scaled, w_key_rope, preferred_element_type=f32)
    squares = jnp.sum(token_rows * token_rows, axis=1)
    sum_q, sum_kv, sum_rope, sum_sq = lax.psum((part_q, part_kv, part_rope, squares), "kv")
    token_scale = lax.rsqrt(sum_sq / D + EPS)[:, None]
    valid_len = prev_len + accepted
    family = ancestry(parents)
    depths = (jnp.sum(family, axis=2) - 1.0).astype(jnp.int32)
    positions = (valid_len[:, None] + depths).reshape(token_count)
    q_norm = normalize(sum_q * token_scale, g_q).astype(bf16)
    q_nope = jnp.dot(
        q_norm, w_up_q.reshape(rank_q, head_count * nope_dim), preferred_element_type=f32
    ).astype(bf16)
    q_nope = q_nope.reshape(token_count, head_count, nope_dim)
    q_absorbed = jnp.einsum("thn,rhn->thr", q_nope, w_up_key, preferred_element_type=f32).astype(
        bf16
    )
    q_raw = jnp.dot(
        q_norm, w_q_rope.reshape(rank_q, head_count * rope_dim), preferred_element_type=f32
    )
    q_rot = rotate(q_raw.reshape(token_count, head_count, rope_dim), positions[:, None]).astype(
        bf16
    )
    latent_new = plain_normalize(sum_kv * token_scale).astype(bf16)
    key_new = rotate(sum_rope * token_scale, positions).astype(bf16)
    offset = lax.axis_index("kv") * span_len
    local_pos = offset + jnp.arange(span_len, dtype=jnp.int32)
    visible = (local_pos[None, :] < valid_len[:, None])[:, None, :]
    query_lat = q_absorbed.reshape(seq_count, prop_count * head_count, rank_kv)
    query_rot = q_rot.reshape(seq_count, prop_count * head_count, rope_dim)
    scores = jnp.einsum("sqr,skr->sqk", query_lat, cache_latent, preferred_element_type=f32)
    scores = (
        scores + jnp.einsum("sqp,skp->sqk", query_rot, cache_rope, preferred_element_type=f32)
    ) * inv_root
    block_peak = jnp.max(jnp.where(visible, scores, NEG_INF), axis=2)
    weights = jnp.where(visible, jnp.exp(scores - block_peak[..., None]), 0.0)
    block_mass = jnp.sum(weights, axis=2)
    block_sum = jnp.einsum(
        "sqk,skr->sqr", weights.astype(bf16), cache_latent, preferred_element_type=f32
    )
    shape_three = (seq_count, prop_count, head_count)
    cache_peak = block_peak.reshape(shape_three)
    cache_mass = block_mass.reshape(shape_three)
    cache_sum = block_sum.reshape(shape_three + (rank_kv,))
    tree_lat = latent_new.reshape(seq_count, prop_count, rank_kv)
    tree_rot = key_new.reshape(seq_count, prop_count, rope_dim)
    lat_four = q_absorbed.reshape(seq_count, prop_count, head_count, rank_kv)
    rot_four = q_rot.reshape(seq_count, prop_count, head_count, rope_dim)
    tree_scores = jnp.einsum("sjhr,skr->sjhk", lat_four, tree_lat, preferred_element_type=f32)
    tree_scores = (
        tree_scores + jnp.einsum("sjhp,skp->sjhk", rot_four, tree_rot, preferred_element_type=f32)
    ) * inv_root
    linked = (family > 0.5)[:, :, None, :]
    tree_peak = jnp.max(jnp.where(linked, tree_scores, NEG_INF), axis=3)
    tree_weights = jnp.where(linked, jnp.exp(tree_scores - tree_peak[..., None]), 0.0)
    tree_mass = jnp.sum(tree_weights, axis=3)
    tree_sum = jnp.einsum(
        "sjhk,skr->sjhr", tree_weights.astype(bf16), tree_lat, preferred_element_type=f32
    )
    up_value = w_up_value.astype(f32)
    cache_vals = jnp.einsum("sjhr,rhv->sjhv", cache_sum, up_value, precision=lax.Precision.HIGHEST)
    tree_vals = jnp.einsum("sjhr,rhv->sjhv", tree_sum, up_value, precision=lax.Precision.HIGHEST)
    merged_all = merged((cache_peak, cache_mass, cache_vals), "kv", blend)
    total_all = blend(merged_all, (tree_peak, tree_mass, tree_vals))
    head_out = total_all[2] / total_all[1][..., None]
    head_rows = head_out.astype(bf16).reshape(token_count, head_count * value_dim)
    group_part = jnp.dot(head_rows, w_out, preferred_element_type=f32)
    mixed_raw = lax.psum(group_part.astype(jnp.bfloat16), "tp").astype(jnp.float32)
    total_sq = lax.psum(jnp.sum(mixed_raw * mixed_raw, axis=1), "kv")
    mixed = mixed_raw * lax.rsqrt(total_sq / D + EPS)[:, None] * g_out.astype(f32)
    mixed = mixed.astype(bf16).reshape(seq_count, prop_count, local_dim)
    slot_hit = (
        local_pos[None, :, None] - valid_len[:, None, None]
        == jnp.arange(prop_count, dtype=jnp.int32)[None, None, :]
    )
    landed = jnp.any(slot_hit, axis=2)[:, :, None]
    placer = slot_hit.astype(bf16)
    placed_lat = jnp.einsum("skj,sjr->skr", placer, tree_lat, preferred_element_type=f32).astype(
        bf16
    )
    placed_rot = jnp.einsum("skj,sjr->skr", placer, tree_rot, preferred_element_type=f32).astype(
        bf16
    )
    new_latent = jnp.where(landed, placed_lat, cache_latent)
    new_rope = jnp.where(landed, placed_rot, cache_rope)
    return (mixed, new_latent, new_rope)


def solution(mesh):
    return jax.shard_map(
        local,
        mesh=mesh,
        in_specs=(
            P("grp", None, "kv"),
            P("grp"),
            P("grp"),
            P("grp", None),
            P("grp", "kv", None),
            P("grp", "kv", None),
            P("kv"),
            P("kv", None),
            P("kv", None),
            P("kv", None),
            P(),
            P(None, "tp", None),
            P(None, "tp", None),
            P(None, "tp", None),
            P(None, "tp", None),
            P("tp", "kv"),
            P("kv"),
        ),
        out_specs=(P("grp", None, "kv"), P("grp", "kv", None), P("grp", "kv", None)),
        check_vma=False,
    )
```

profile of v0, /device:TPU:0, one launch (start us, length us, event | category | flops | bytes accessed | tf_op | source)
XLA Modules:
  0.0 125.8 jit_solution(11165840684787897321)
XLA Ops:
  7.3 0.8 convert_element_type.117
  8.1 0.8 reshape.274
  8.8 0.8 fusion.74
  9.7 0.9 multiply_reduce_fusion.1
  10.6 0.8 copy.99
  11.4 0.7 add.198
  12.5 0.3 broadcast_compare_fusion
  13.4 21.6 %all-reduce = (f32[32]{0:T(128)S(1)}, f32[32,256]{1,0:T(8,128)S(1)}, f32[32,64]{1,0:T(8,128)S(1)}) all-reduce(f32[32]{0:T(128)S(1)} %reduce_sum.66, f32[32,256]{1,0:T(8,128)S(1)} %fusion.75, f32[32,64]{1,0:T(8,128)S(1)} %fusion.76), channel_id=1, replica_groups=mesh['grp'=2,'kv'=4,'tp'=4] {'kv'}, use_global_device_ids=true, to_apply=%region_2.0 | all-reduce | flops 10272 | bytes 82176 | tf_op jit(solution)/shard_map/psum | solution.py:110
  35.6 1.6 %fusion.4 = bf16[8,256,256]{2,1,0:T(8,128)(2,1)} fusion(bf16[8,256,256]{2,1,0:T(8,128)(2,1)S(1)} %copy-done.1, bf16[8,4,256]{2,1,0:T(4,128)(2,1)S(1)} %reshape.271, pred[8,256]{1,0:T(8,128)(4,1)S(1)} %fusion.49, s32[8,256]{1,0:T(8,128)S(1)} %broadcast_subtract_fusion), kind=kOutput, calls=%fused_computation.11 | convolution fusion | flops 5251072 | bytes 2123776 | tf_op jit(solution)/shard_map/skj,sjr->skr/dot_general | solution.py:184
  37.2 1.0 fusion.5
  38.5 9.1 %all-reduce.3.cloned.1.call-done = f32[32,512]{1,0:T(8,128)} async-done(((f32[32,512]{1,0:T(8,128)}), f32[32,512]{1,0:T(8,128)}) %all-reduce.3.cloned.1.call-update) | async-done | bytes 65552 | tf_op jit(solution)/shard_map/psum | solution.py:110
  47.6 1.0 multiply_reduce_fusion
  48.6 1.1 fusion.17
  49.9 1.1 fusion.12
  51.5 0.5 select_reduce_fusion
  52.6 0.5 fusion.44
  54.0 13.1 %all_gather.13 = f32[4,8,4,4]{1,3,2,0:T(4,128)S(1)} all-gather(f32[1,8,4,4]{1,3,2,0:T(4,128)S(1)} %bitcast.127), channel_id=1, replica_groups=mesh['grp'=2,'kv'=4,'tp'=4] {'kv'}, dimensions={0}, use_global_device_ids=true | all-gather | bytes 2560 | tf_op jit(solution)/shard_map/all_gather | solution.py:15
  67.1 13.2 %all_gather.12 = f32[4,8,4,4]{1,3,2,0:T(4,128)S(1)} all-gather(f32[1,8,4,4]{1,3,2,0:T(4,128)S(1)} %bitcast.123), channel_id=1, replica_groups=mesh['grp'=2,'kv'=4,'tp'=4] {'kv'}, dimensions={0}, use_global_device_ids=true | all-gather | bytes 2560 | tf_op jit(solution)/shard_map/all_gather | solution.py:15
  80.7 13.8 %all-gather = f32[32,4,4,128]{3,0,1,2:T(8,128)S(1)} all-gather(f32[8,4,4,128]{3,0,1,2:T(8,128)S(1)} %convolution_bitcast_fusion.1), channel_id=2, replica_groups=mesh['grp'=2,'kv'=4,'tp'=4] {'kv'}, dimensions={0}, use_global_device_ids=true | all-gather | bytes 327680 | tf_op jit(solution)/shard_map/all_gather | solution.py:15
  94.5 1.5 %while.19 = (s32[]{:T(128)}, f32[8,4,4]{0,2,1:T(4,128)S(1)}, f32[8,4,4]{0,2,1:T(4,128)S(1)}, f32[8,4,4,128]{3,2,1,0:T(4,128)S(1)}, f32[4,8,4,4]{1,3,2,0:T(4,128)...) while((s32[]{:T(128)}, f32[8,4,4]{0,2,1:T(4,128)S(1)}, ...), condition=%wide.region_8.9_spmd, body=%wide.region_7.0_spmd.sunk | while | flops 49925 | bytes 334991 | solution.py:20
  96.5 0.6 copy-done.3
  97.3 10.3 %psum.46 = bf16[32,512]{1,0:T(8,128)(2,1)S(1)} all-reduce(bf16[32,512]{1,0:T(8,128)(2,1)S(1)} %convolution_convert_fusion.3), channel_id=1, replica_groups=mesh['grp'=2,'kv'=4,'tp'=4] {'tp'}, use_global_device_ids=true, to_apply=%region_14.15 | all-reduce | flops 16384 | bytes 65536 | tf_op jit(solution)/shard_map/psum | solution.py:174
  107.7 10.6 %psum.47 = f32[32]{0:T(128)S(1)} all-reduce(f32[32]{0:T(128)S(1)} %fusion.26), channel_id=1, replica_groups=mesh['grp'=2,'kv'=4,'tp'=4] {'kv'}, use_global_device_ids=true, to_apply=%region_16.17 | all-reduce | flops 32 | bytes 256 | tf_op jit(solution)/shard_map/psum | solution.py:175
  118.3 0.6 reshape.273
  (102 shorter events, 6.7 us)
Async XLA Ops:
  7.2 1.7 %copy-start = (bf16[512,512]{1,0:T(8,128)(2,1)S(1)}, bf16[512,512]{1,0:T(8,128)(2,1)}, u32[]{:S(2)}) copy-start(bf16[512,512]{1,0:T(8,128)(2,1)} %param.26) | copy-start | bytes 1572868
  7.2 5.9 %copy-start.8 = (bf16[512,64]{0,1:T(8,128)(2,1)S(1)}, bf16[512,64]{0,1:T(8,128)(2,1)}, u32[]{:S(2)}) copy-start(bf16[512,64]{0,1:T(8,128)(2,1)} %param.28) | copy-start | bytes 196612
  7.2 6.0 %copy-start.4 = (bf16[512,256]{1,0:T(8,128)(2,1)S(1)}, bf16[512,256]{1,0:T(8,128)(2,1)}, u32[]{:S(2)}) copy-start(bf16[512,256]{1,0:T(8,128)(2,1)} %param.27) | copy-start | bytes 786436
  7.2 28.4 %copy-start.1 = (bf16[8,256,256]{2,1,0:T(8,128)(2,1)S(1)}, bf16[8,256,256]{2,1,0:T(8,128)(2,1)}, u32[]{:S(2)}) copy-start(bf16[8,256,256]{2,1,0:T(8,128)(2,1)} %param.23) | copy-start | bytes 3145732
  7.2 40.4 %all-reduce.3.cloned.1.call-start = ((), (), s32[]{:S(2)}) async-start(), calls=%async_computation | async-start | bytes 131072 | tf_op jit(solution)/shard_map/psum | solution.py:110
  35.6 1.6 %copy-start.2 = (bf16[8,256,64]{1,2,0:T(8,128)(2,1)S(1)}, bf16[8,256,64]{1,2,0:T(8,128)(2,1)}, u32[]{:S(2)}) copy-start(bf16[8,256,64]{1,2,0:T(8,128)(2,1)} %param.24) | copy-start | bytes 786436
  35.6 2.8 %copy-start.9 = (bf16[512]{0:T(512)(128)(2,1)S(1)}, bf16[512]{0:T(512)(128)(2,1)}, u32[]{:S(2)}) copy-start(bf16[512]{0:T(512)(128)(2,1)} %param.29) | copy-start | bytes 3076
  35.6 2.8 %copy-start.10 = (bf16[512]{0:T(512)(128)(2,1)S(1)}, bf16[512]{0:T(512)(128)(2,1)}, u32[]{:S(2)}) copy-start(bf16[512]{0:T(512)(128)(2,1)} %param.35) | copy-start | bytes 3076
  35.6 13.0 %copy-start.6 = (bf16[512,4,64]{0,2,1:T(8,128)(2,1)S(1)}, bf16[512,4,64]{0,2,1:T(8,128)(2,1)}, u32[]{:S(2)}) copy-start(bf16[512,4,64]{0,2,1:T(8,128)(2,1)} %param.31) | copy-start | bytes 786436
  37.2 12.7 %copy-start.11 = (bf16[512,4,128]{2,1,0:T(4,128)(2,1)S(1)}, bf16[512,4,128]{2,1,0:T(4,128)(2,1)}, u32[]{:S(2)}) copy-start(bf16[512,4,128]{2,1,0:T(4,128)(2,1)} %param.30) | copy-start | bytes 1572868
  37.2 13.8 %copy-start.7 = (bf16[256,4,128]{2,1,0:T(4,128)(2,1)S(1)}, bf16[256,4,128]{2,1,0:T(4,128)(2,1)}, u32[]{:S(2)}) copy-start(bf16[256,4,128]{2,1,0:T(4,128)(2,1)} %param.32) | copy-start | bytes 786436
  52.4 27.9 %copy-start.5 = (bf16[256,4,128]{2,1,0:T(4,128)(2,1)S(1)}, bf16[256,4,128]{2,1,0:T(4,128)(2,1)}, u32[]{:S(2)}) copy-start(bf16[256,4,128]{2,1,0:T(4,128)(2,1)} %param.33) | copy-start | bytes 786436
  96.1 1.0 copy-start.3
Sparse Core Ops, SparseCore 0:
  10.3 37.2 all-reduce.2
where the time goes:
time: 126 us
  blocking collectives  82.5 us (65%)
  between operations  14.4 us (11%)
  matrix products  9.17 us (7%)
  waiting for transfers between devices  9.1 us (7%)
  other arithmetic  5.63 us (4%)
  local copies, waits for them, and re-layouts  4.86 us (4%)
    all_gather x3, blocking collectives, merged(): gathered = jax.tree.map(lambda a: lax.all_gather(a, axis), part)  40.1 us
    psum x1, blocking collectives, local(): lax.psum((part_q, part_kv, part_rope, squares), 'kv')  21.6 us
    psum x1, blocking collectives, local(): total_sq = lax.psum(jnp.sum(mixed_raw * mixed_raw, axis=1), 'kv')  10.6 us
    psum x1, blocking collectives, local(): lax.psum(group_part.astype(jnp.bfloat16), 'tp').astype(jnp.float32)  10.3 us
    psum x1, waiting for transfers between devices, local(): lax.psum((part_q, part_kv, part_rope, squares), 'kv')  9.08 us
  transfers between devices with their start and end apart: 1, of which 1 were waited for; matrix products, arithmetic and copies ran while one was open for 6% of the time, Pallas kernels for 0%

commit v1 on v0

v1 whole, which is shorter than its diff:
```python
import functools

import jax
import jax.numpy as jnp
from jax import lax
from jax.experimental import pallas as pl
from jax.experimental.pallas import tpu as pltpu
from jax.sharding import PartitionSpec as P

EPS = 1e-06
ROPE_BASE = 10000.0
NEG_INF = -1e30
LANES = 128
F32 = jnp.float32
BF16 = jnp.bfloat16
NT = (((1,), (1,)), ((), ()))


def dot(a, b):
    return jnp.dot(a, b, preferred_element_type=F32)


def dot_nt(a, b):
    return lax.dot_general(a, b, NT, preferred_element_type=F32)


def rotated(x, cosine, sine, rope):
    width = x.shape[1]
    lane = lax.broadcasted_iota(jnp.int32, x.shape, 1)
    front = lax.rem(lane, rope) < rope // 2
    partner = jnp.where(front, -pltpu.roll(x, width - rope // 2, 1), pltpu.roll(x, rope // 2, 1))
    return x * cosine + partner * sine


def column_to_row(column):
    rows = column.shape[0]
    wide = jnp.broadcast_to(column, (rows, LANES))
    if rows < LANES:
        wide = jnp.concatenate([wide, jnp.zeros((LANES - rows, LANES), F32)], axis=0)
    return wide.T[0:1, :]


def kernel(
    nk, nt, seqs, props, heads, qr, kvr, rope, vd, nope, model,
    valid_ref, tokens_ref, g_pre_ref, g_q_ref, g_out_ref, table_ref, mask_ref,
    wdq_hbm, wdkv_hbm, wkr_hbm, wuq_hbm, wqr_hbm, wuk_hbm, wuv_hbm, wout_hbm, lat_hbm, rot_hbm,
    mixed_ref, latnew_ref, keynew_ref,
    wdq, wdkv, wkr, wuq, wqr, wuk, wuv, wout, lat, rot,
    tok, buf1, buf2, buf3, lse3, buf4, buf5, qa, cs,
    load_sem, send1, recv1, send2, recv2, send3, recv3, send3b, recv3b, send4, recv4, send5, recv5,
):
    me_k = lax.axis_index("kv")
    me_t = lax.axis_index("tp")
    tokens = seqs * props
    group = tokens // nt
    rows = heads * tokens
    span = lat.shape[1]
    per_seq = heads * props

    barrier = pltpu.get_barrier_semaphore()
    for d in range(1, nk):
        pl.semaphore_signal(barrier, inc=1, device_id={"kv": lax.rem(me_k + d, nk)})
    for d in range(1, nt):
        pl.semaphore_signal(barrier, inc=1, device_id={"tp": lax.rem(me_t + d, nt)})

    loads = []
    for i, (src, dst) in enumerate(
        (
            (wdq_hbm, wdq), (wdkv_hbm, wdkv), (wkr_hbm, wkr), (wuq_hbm, wuq), (wqr_hbm, wqr),
            (wuk_hbm, wuk), (lat_hbm, lat), (rot_hbm, rot), (wuv_hbm, wuv), (wout_hbm, wout),
        )
    ):
        copy = pltpu.make_async_copy(src, dst, load_sem.at[i])
        copy.start()
        loads.append(copy)

    def exchange(buffer, axis, me, n, send, recv):
        copies = []
        for d in range(1, n):
            copy = pltpu.make_async_remote_copy(
                src_ref=buffer.at[me],
                dst_ref=buffer.at[me],
                send_sem=send.at[d - 1],
                recv_sem=recv.at[d - 1],
                device_id={axis: lax.rem(me + d, n)},
                device_id_type=pl.DeviceIdType.MESH,
            )
            copy.start()
            copies.append(copy)
        return copies

    sent = []

    tok[...] = tokens_ref[...].astype(F32)
    x = tok[pl.ds(pl.multiple_of(me_t * group, group), group), :]
    scaled = (x * g_pre_ref[...].astype(F32)).astype(BF16)
    squares = jnp.sum(x * x, axis=1, keepdims=True)
    for i in range(3):
        loads[i].wait()
    buf1[me_k, :, 0:qr] = dot(scaled, wdq[...])
    buf1[me_k, :, qr : qr + kvr] = dot(scaled, wdkv[...])
    buf1[me_k, :, qr + kvr : qr + kvr + LANES] = jnp.concatenate(
        [dot(scaled, wkr[...]), jnp.broadcast_to(squares, (group, LANES - rope))], axis=1
    )
    pl.semaphore_wait(barrier, nk - 1 + nt - 1)
    copies = exchange(buf1, "kv", me_k, nk, send1, recv1)
    sent += copies
    for copy in copies:
        copy.wait_recv()
    total = buf1[0]
    for k in range(1, nk):
        total = total + buf1[k]
    last = total[:, qr + kvr :]
    scale = lax.rsqrt(last[:, rope : rope + 1] / model + EPS)
    q_latent = total[:, 0:qr] * scale
    q_norm = (
        q_latent
        * lax.rsqrt(jnp.mean(q_latent * q_latent, axis=1, keepdims=True) + EPS)
        * g_q_ref[...].astype(F32)
    )
    kv_latent = total[:, qr : qr + kvr] * scale
    latent = kv_latent * lax.rsqrt(jnp.mean(kv_latent * kv_latent, axis=1, keepdims=True) + EPS)
    table = table_ref[pl.ds(pl.multiple_of(me_t * group, group), group), :]
    key = rotated(last * scale, table[:, 0:LANES], table[:, LANES:], rope)
    buf2[me_t, :, 0:qr] = q_norm.astype(BF16)
    buf2[me_t, :, qr : qr + kvr] = latent.astype(BF16)
    buf2[me_t, :, qr + kvr :] = key.astype(BF16)
    copies = exchange(buf2, "tp", me_t, nt, send2, recv2)
    sent += copies
    for i in range(3, 8):
        loads[i].wait()
    for copy in copies:
        copy.wait_recv()

    gathered = buf2[...].astype(F32).reshape(tokens, qr + kvr + LANES)
    q_all = gathered[:, 0:qr].astype(BF16)
    lat_new = gathered[:, qr : qr + kvr].astype(BF16)
    key_new = gathered[:, qr + kvr : qr + kvr + rope].astype(BF16)
    latnew_ref[...] = lat_new
    keynew_ref[...] = key_new

    q_nope = dot(q_all, wuq[...]).astype(BF16)
    q_raw = dot(q_all, wqr[...])
    copies_wide = heads * rope // LANES
    cosine = jnp.concatenate([table_ref[:, 0:LANES]] * copies_wide, axis=1)
    sine = jnp.concatenate([table_ref[:, LANES:]] * copies_wide, axis=1)
    q_rot = rotated(q_raw, cosine, sine, rope)
    lat_tiles = kvr // LANES
    for h in range(heads):
        part = dot_nt(
            q_nope[:, h * nope : (h + 1) * nope], wuk[:, h * nope : (h + 1) * nope]
        )
        for c in range(lat_tiles):
            qa[c, h * tokens : (h + 1) * tokens, :] = part[:, c * LANES : (c + 1) * LANES]
        qa[lat_tiles, h * tokens : (h + 1) * tokens, 0:rope] = q_rot[:, h * rope : (h + 1) * rope]

    inv_root = (nope + rope) ** (-0.5)
    offset = me_k * span
    column = lax.broadcasted_iota(jnp.int32, (per_seq, span), 1) + offset
    for s in range(seqs):
        pick = pl.ds(s, per_seq, stride=seqs)
        q_lat = jnp.concatenate([qa[c, pick, :] for c in range(lat_tiles)], axis=1).astype(BF16)
        q_pos = qa[lat_tiles, pick, :][:, 0:rope].astype(BF16)
        scores = (dot_nt(q_lat, lat[s]) + dot_nt(q_pos, rot[s])) * inv_root
        seen = column < valid_ref[s]
        peak = jnp.max(jnp.where(seen, scores, NEG_INF), axis=1, keepdims=True)
        weights = jnp.where(seen, jnp.exp(scores - peak), 0.0)
        mass = jnp.sum(weights, axis=1, keepdims=True)
        some = mass > 0.0
        safe = jnp.where(some, mass, 1.0)
        mean = dot(weights.astype(BF16), lat[s]) / safe
        lse = jnp.where(some, peak + jnp.log(safe), NEG_INF)
        for c in range(lat_tiles):
            cs[c, pick, :] = mean[:, c * LANES : (c + 1) * LANES]
        cs[lat_tiles, pick, :] = jnp.broadcast_to(lse, (per_seq, LANES))

    loads[8].wait()

    def up_value(means, h):
        high = means.astype(BF16)
        low = (means - high.astype(F32)).astype(BF16)
        weight = wuv[:, h * vd : (h + 1) * vd]
        return dot(high, weight) + dot(low, weight)

    for h in range(heads):
        rows_h = slice(h * tokens, (h + 1) * tokens)
        means = jnp.concatenate([cs[c, rows_h, :] for c in range(lat_tiles)], axis=1)
        buf3[me_k, rows_h, :] = up_value(means, h).astype(BF16)
    lse3[me_k] = cs[lat_tiles].T[0:1, :]
    copies = exchange(lse3, "kv", me_k, nk, send3b, recv3b)
    copies += exchange(buf3, "kv", me_k, nk, send3, recv3)
    sent += copies

    q_lat = jnp.concatenate([qa[c] for c in range(lat_tiles)], axis=1).astype(BF16)
    q_pos = qa[lat_tiles][:, 0:rope].astype(BF16)
    scores = (dot_nt(q_lat, lat_new) + dot_nt(q_pos, key_new)) * inv_root
    linked = jnp.concatenate([mask_ref[...]] * heads, axis=0) > 0.5
    peak = jnp.max(jnp.where(linked, scores, NEG_INF), axis=1, keepdims=True)
    weights = jnp.where(linked, jnp.exp(scores - peak), 0.0)
    mass = jnp.sum(weights, axis=1, keepdims=True)
    means = dot(weights.astype(BF16), lat_new) / mass
    tree_lse = peak + jnp.log(mass)
    tree_vals = jnp.concatenate(
        [up_value(means[h * tokens : (h + 1) * tokens], h) for h in range(heads)], axis=0
    )
    loads[9].wait()
    for copy in copies:
        copy.wait_recv()

    padding = jnp.full((LANES - nk, LANES), NEG_INF, F32)
    lses = jnp.concatenate([lse3[k] for k in range(nk)] + [padding], axis=0).T
    top = jnp.maximum(jnp.max(lses, axis=1, keepdims=True), tree_lse)
    share = jnp.exp(lses - top)
    tree_share = jnp.exp(tree_lse - top)
    divisor = jnp.sum(share, axis=1, keepdims=True) + tree_share
    merged = tree_share * tree_vals
    for k in range(nk):
        merged = merged + share[:, k : k + 1] * buf3[k].astype(F32)
    head_out = (merged / divisor).astype(BF16)
    head_rows = jnp.concatenate(
        [head_out[h * tokens : (h + 1) * tokens] for h in range(heads)], axis=1
    )
    buf4[me_t] = dot(head_rows, wout[...]).astype(BF16)
    copies = exchange(buf4, "tp", me_t, nt, send4, recv4)
    sent += copies
    for copy in copies:
        copy.wait_recv()
    mixed_raw = buf4[0].astype(F32)
    for t in range(1, nt):
        mixed_raw = mixed_raw + buf4[t].astype(F32)
    buf5[me_k] = column_to_row(jnp.sum(mixed_raw * mixed_raw, axis=1, keepdims=True))
    copies = exchange(buf5, "kv", me_k, nk, send5, recv5)
    sent += copies
    scaled_out = mixed_raw * g_out_ref[...].astype(F32)
    for copy in copies:
        copy.wait_recv()
    total_sq = buf5[0]
    for k in range(1, nk):
        total_sq = total_sq + buf5[k]
    factor = lax.rsqrt(total_sq / model + EPS)
    factor = jnp.broadcast_to(factor, (LANES, LANES)).T[0:tokens, 0:1]
    mixed_ref[...] = (scaled_out * factor).astype(BF16)
    for copy in sent:
        copy.wait_send()


def lineage(parents):
    props = parents.shape[1]
    index = jnp.arange(props, dtype=jnp.int32)
    rows = []
    for j in range(props):
        row = jnp.broadcast_to(index == j, (parents.shape[0], props))
        for m in range(j):
            row = row | ((parents[:, j : j + 1] == m) & rows[m])
        rows.append(row)
    return jnp.stack(rows, axis=1)


def local(
    nk,
    nt,
    tokens,
    prev_len,
    accepted,
    parents,
    cache_latent,
    cache_rope,
    g_pre,
    w_down_q,
    w_down_kv,
    w_key_rope,
    g_q,
    w_up_q,
    w_q_rope,
    w_up_key,
    w_up_value,
    w_out,
    g_out,
):
    seqs, props, width = tokens.shape
    count = seqs * props
    group = count // nt
    qr, heads, nope = w_up_q.shape
    rope = w_q_rope.shape[2]
    kvr = w_up_key.shape[0]
    vd = w_up_value.shape[2]
    span = cache_latent.shape[1]
    width_out = w_out.shape[1]
    rows = heads * count
    wide = qr + kvr + LANES

    valid_len = prev_len + accepted
    family = lineage(parents)
    depths = jnp.sum(family.astype(jnp.int32), axis=2) - 1
    positions = (valid_len[:, None] + depths).T.reshape(count)
    half = rope // 2
    frequency = ROPE_BASE ** (-jnp.arange(half, dtype=F32) / half)
    angles = positions.astype(F32)[:, None] * jnp.tile(frequency, LANES // half)
    table = jnp.concatenate([jnp.cos(angles), jnp.sin(angles)], axis=1)
    same = jnp.eye(seqs, dtype=F32)
    mask = (family.astype(F32).transpose(1, 0, 2)[:, :, :, None] * same[None, :, None, :]).reshape(
        count, count
    )
    rows_in = tokens.transpose(1, 0, 2).reshape(count, width)

    vmem = pl.BlockSpec(memory_space=pltpu.VMEM)
    anywhere = pl.BlockSpec(memory_space=pl.ANY)
    dma = pltpu.SemaphoreType.DMA
    weights = (
        w_down_q,
        w_down_kv,
        w_key_rope,
        w_up_q.reshape(qr, heads * nope),
        w_q_rope.reshape(qr, heads * rope),
        w_up_key.reshape(kvr, heads * nope),
        w_up_value.reshape(kvr, heads * vd),
        w_out,
        cache_latent,
        cache_rope,
    )
    mixed, lat_new, key_new = pl.pallas_call(
        functools.partial(
            kernel, nk, nt, seqs, props, heads, qr, kvr, rope, vd, nope, width * nk
        ),
        out_shape=(
            jax.ShapeDtypeStruct((count, width_out), BF16),
            jax.ShapeDtypeStruct((count, kvr), BF16),
            jax.ShapeDtypeStruct((count, rope), BF16),
        ),
        in_specs=[pl.BlockSpec(memory_space=pltpu.SMEM)] + [vmem] * 6 + [anywhere] * 10,
        out_specs=(vmem, vmem, vmem),
        scratch_shapes=[pltpu.VMEM(w.shape, BF16) for w in weights]
        + [
            pltpu.VMEM((count, width), F32),
            pltpu.VMEM((nk, group, wide), F32),
            pltpu.VMEM((nt, group, wide), BF16),
            pltpu.VMEM((nk, rows, vd), BF16),
            pltpu.VMEM((nk, 1, LANES), F32),
            pltpu.VMEM((nt, count, width_out), BF16),
            pltpu.VMEM((nk, 1, LANES), F32),
            pltpu.VMEM((kvr // LANES + 1, rows, LANES), F32),
            pltpu.VMEM((kvr // LANES + 1, rows, LANES), F32),
            dma((10,)),
            dma((nk - 1,)),
            dma((nk - 1,)),
            dma((nt - 1,)),
            dma((nt - 1,)),
            dma((nk - 1,)),
            dma((nk - 1,)),
            dma((nk - 1,)),
            dma((nk - 1,)),
            dma((nt - 1,)),
            dma((nt - 1,)),
            dma((nk - 1,)),
            dma((nk - 1,)),
        ],
        compiler_params=pltpu.CompilerParams(collective_id=0, has_side_effects=True),
    )(
        valid_len,
        rows_in,
        g_pre.reshape(1, width),
        g_q.reshape(1, qr),
        g_out.reshape(1, width_out),
        table,
        mask,
        *weights,
    )

    slot = (
        lax.axis_index("kv") * span
        + jnp.arange(span, dtype=jnp.int32)[None, :]
        - valid_len[:, None]
    )[:, :, None]
    new_latent = cache_latent
    new_rope = cache_rope
    for j in range(props):
        here = slot == j
        new_latent = jnp.where(here, lat_new[j * seqs : (j + 1) * seqs, None, :], new_latent)
        new_rope = jnp.where(here, key_new[j * seqs : (j + 1) * seqs, None, :], new_rope)
    return (
        mixed.reshape(props, seqs, width_out).transpose(1, 0, 2),
        new_latent,
        new_rope,
    )


def solution(mesh):
    return jax.shard_map(
        functools.partial(local, mesh.shape["kv"], mesh.shape["tp"]),
        mesh=mesh,
        in_specs=(
            P("grp", None, "kv"),
            P("grp"),
            P("grp"),
            P("grp", None),
            P("grp", "kv", None),
            P("grp", "kv", None),
            P("kv"),
            P("kv", None),
            P("kv", None),
            P("kv", None),
            P(),
            P(None, "tp", None),
            P(None, "tp", None),
            P(None, "tp", None),
            P(None, "tp", None),
            P("tp", "kv"),
            P("kv"),
        ),
        out_specs=(P("grp", None, "kv"), P("grp", "kv", None), P("grp", "kv", None)),
        check_vma=False,
    )
```

time: 126 us -> 48.6 us (0.39)
  blocking collectives: 82.5 us -> 0 us
  Pallas kernels: 0 us -> 29.3 us
  between operations: 14.4 us -> 0.7 us
  matrix products: 9.17 us -> 0 us
  waiting for transfers between devices: 9.1 us -> 0 us
  local copies, waits for them, and re-layouts: 4.86 us -> 12.2 us
    psum x3 -> x0, blocking collectives: 42.5 us -> none  [the longest x1 21.6 us: local(): lax.psum((part_q, part_kv, part_rope, squares), 'kv')]
    all_gather x3 -> x0, blocking collectives: 40.1 us -> none  [merged(): gathered = jax.tree.map(lambda a: lax.all_gather(a, axis), part)]
    pallas_call x0 -> x1, Pallas kernels: none -> 29.3 us  [local(): pl.pallas_call(functools.partial(kernel, nk, nt, seqs, props, heads, qr,...]
    dot_general x19 -> x0, matrix products: 9.17 us -> none  [the longest x1 1.58 us: local(): jnp.einsum('skj,sjr->skr', placer, tree_lat, preferred_element_type=f32)]
    psum x1 -> x0, waiting for transfers between devices: 9.08 us -> none  [local(): lax.psum((part_q, part_kv, part_rope, squares), 'kv')]
    reshape x5 -> x6, local copies, waits for them, and re-layouts: 0.73 us -> 5.1 us  [the longest x1 1.86 us: local(): w_up_value.reshape(kvr, heads * vd)]
    select_n x0 -> x2, other arithmetic: none -> 3.51 us  [the longest x1 2.47 us: local(): jnp.where(here, lat_new[j * seqs:(j + 1) * seqs, None, :], new_latent)]
    unnamed x25 -> x31, local copies, waits for them, and re-layouts: 1.47 us -> 4.75 us
  transfers between devices with their start and end apart: 1 -> 0, of which waited for: 1 -> 0; matrix products, arithmetic and copies ran while one was open for 6% -> 0% of each run, Pallas kernels for 0% -> 0%
where the time goes in v1:
time: 48.6 us; the launch traced here: 48.2 us
  Pallas kernels  29.3 us (60%)
  local copies, waits for them, and re-layouts  12.2 us (25%)
  other arithmetic  6.06 us (12%)
  between operations  0.7 us (1%)
    pallas_call x1, Pallas kernels, local(): pl.pallas_call(functools.partial(kernel, nk, nt, seqs, props, heads, qr,...  29.3 us
    unnamed x31, local copies, waits for them, and re-layouts  4.75 us
    select_n x1, other arithmetic, local(): jnp.where(here, lat_new[j * seqs:(j + 1) * seqs, None, :], new_latent)  2.47 us
    reshape x1, local copies, waits for them, and re-layouts, local(): w_up_value.reshape(kvr, heads * vd)  1.86 us
    select_n x1, other arithmetic, local(): jnp.where(here, key_new[j * seqs:(j + 1) * seqs, None, :], new_rope)  1.04 us

profile of v1, /device:TPU:0, one launch (start us, length us, event | category | flops | bytes accessed | tf_op | source)
XLA Modules:
  0.0 48.2 jit_solution(11656820478131957651)
XLA Ops:
  0.6 0.8 %compare_bitcast_fusion.5 = (pred[8]{0:T(512)(128)(4,1)S(1)}, pred[8]{0:T(512)(128)(4,1)S(1)}, pred[8]{0:T(512)(128)(4,1)S(1)}, pred[8]{0:T(512)(128)(4,1)S(1)},...) fusion(s32[8,4]{0,1:T(4,128)} %param.20), kind=kLoop, calls=%fused_computation.29 | loop fusion | flops 48 | bytes 144 | tf_op jit(solution)/shard_map/eq | solution.py:254
  1.6 0.1 copy.31
  1.7 0.1 broadcast_multiply_fusion
  1.8 0.7 %mul.42.mask_ref = f32[32,32]{1,0:T(8,128)} reshape(f32[4,8,4,8]{3,2,1,0:T(4,128)S(1)} %broadcast_multiply_fusion) | data formatting | bytes 8192 | tf_op jit(solution)/shard_map/mul | solution.py:301
  2.6 0.7 %add.27.valid_ref = s32[8]{0:T(128)S(1)} add(s32[8]{0:T(128)} %param.18, s32[8]{0:T(128)} %param.19) | non-fusion elementwise | flops 8 | bytes 96 | tf_op jit(solution)/shard_map/add | solution.py:292
  3.2 0.5 %copy-done.9 = s32[8]{0:T(128)} copy-done((s32[8]{0:T(128)}, s32[8]{0:T(128)S(1)}, u32[]{:S(2)}) %copy-start.9) | copy-done | bytes 56
  4.0 0.1 multiply_cosine_fusion
  4.1 0.6 %pad_maximum_fusion.table_ref = f32[32,256]{1,0:T(8,128)} fusion(f32[32,128]{1,0:T(8,128)S(1)} %get-tuple-element.31, f32[32,128]{1,0:T(8,128)S(1)} %get-tuple-element.30), kind=kLoop, calls=%fused_computation.5 | loop fusion | flops 8192 | bytes 65536 | tf_op jit(solution)/shard_map/concatenate | solution.py:299
  4.7 1.9 %copy_bitcast_fusion.1 = (bf16[256,512]{1,0:T(8,128)(2,1)}, bf16[256,512]{1,0:T(8,128)(2,1)}) fusion(bf16[32,8,4,128]{3,2,1,0:T(4,128)(2,1)S(1)} %bitcast.38, bf16[32,8,4,128]{3,2,1,0:T(4,128)(2,1)} %bitcast.39), kind=kLoop, calls=%fused_computation.2 | loop fusion | bytes 1048576 | tf_op jit(solution)/shard_map/reshape | solution.py:316
  6.6 0.9 %copy.44 = bf16[64,8,4,128]{3,1,2,0:T(8,128)(2,1)} copy(bf16[64,8,4,128]{3,2,1,0:T(4,128)(2,1)S(1)} %bitcast.36) | data formatting | bytes 1048576
  7.5 1.0 %copy.34.rot_hbm = bf16[8,256,64]{2,1,0:T(8,128)(2,1)} copy(bf16[8,256,64]{1,2,0:T(8,128)(2,1)S(1)} %copy-done.1) | data formatting | bytes 524288 | tf_op args[5]
  8.6 0.8 %copy.33.wqr_hbm = bf16[512,256]{1,0:T(8,128)(2,1)} copy(bf16[512,256]{0,1:T(8,128)(2,1)S(1)} %bitcast.37) | data formatting | bytes 524288 | tf_op jit(solution)/shard_map/reshape | solution.py:314
  9.4 0.8 %copy.32.wkr_hbm = bf16[512,64]{1,0:T(8,128)(2,1)} copy(bf16[512,64]{0,1:T(8,128)(2,1)S(1)} %copy-done.5) | data formatting | bytes 131072 | tf_op args[9]
  10.2 0.6 %copy.46 = bf16[4,8,512]{2,1,0:T(8,128)(2,1)} copy(bf16[4,8,512]{2,0,1:T(4,128)(2,1)S(1)} %bitcast.41) | data formatting | bytes 65536 | tf_op jit(solution)/shard_map/transpose | solution.py:304
  10.8 0.7 %copy-done.11 = bf16[512]{0:T(512)(128)(2,1)S(1)} copy-done((bf16[512]{0:T(512)(128)(2,1)S(1)}, bf16[512]{0:T(512)(128)(2,1)}, u32[]{:S(2)}) %copy-start.11) | copy-done | bytes 1048
  11.5 0.6 %reshape.652.g_pre_ref = bf16[1,512]{1,0:T(2,128)(2,1)} reshape(bf16[512]{0:T(512)(128)(2,1)S(1)} %copy-done.11) | data formatting | bytes 2048 | tf_op jit(solution)/shard_map/reshape | solution.py:361
  12.1 0.6 %reshape.653.g_q_ref = bf16[1,512]{1,0:T(2,128)(2,1)} reshape(bf16[512]{0:T(512)(128)(2,1)S(1)} %copy-done.12) | data formatting | bytes 2048 | tf_op jit(solution)/shard_map/reshape | solution.py:362
  12.8 0.6 %reshape.654.g_out_ref = bf16[1,512]{1,0:T(2,128)(2,1)} reshape(bf16[512]{0:T(512)(128)(2,1)S(1)} %copy-done.13) | data formatting | bytes 2048 | tf_op jit(solution)/shard_map/reshape | solution.py:363
  13.4 29.3 %shard_map.184 = (bf16[32,512]{1,0:T(8,128)(2,1)}, bf16[32,256]{1,0:T(8,128)(2,1)}, bf16[32,64]{1,0:T(8,128)(2,1)}) custom-call(s32[8]{0:T(128)} %copy-done.9, bf16[32,512]{1,0:T(8,128)(2,1)} %bitcast.40, bf16[1,512]{1,0:T(2,128)(2,1)} %reshape.652.g_pre_ref, bf16[1,512]{1,0:T(2,128)(2,1)} %reshape.653.g_q_ref, bf16[1,512]{1,0:T(2,128)(2,1)} %reshape.654.g_out_ref, ...), custom_call_target="tpu_custom_call" | custom-call | tf_op jit(solution)/shard_map/pallas_call | solution.py:321
  42.7 0.7 %fusion.2 = (bf16[8,64]{1,0:T(8,128)(2,1)S(1)}, bf16[8,64]{1,0:T(8,128)(2,1)S(1)}, bf16[8,64]{1,0:T(8,128)(2,1)S(1)}, bf16[8,64]{1,0:T(8,128)(2,1)S(1)}) fusion(bf16[32,64]{1,0:T(8,128)(2,1)} %get-tuple-element.8), kind=kLoop, calls=%fused_computation.37 | loop fusion | bytes 8192 | tf_op jit(solution)/shard_map/slice | solution.py:379
  43.4 0.6 %copy-done.10 = s32[8]{0:T(128)S(1)} copy-done((s32[8]{0:T(128)S(1)}, s32[8]{0:T(128)}, u32[]{:S(2)}) %copy-start.10) | copy-done | bytes 56
  44.1 1.0 %select_select_fusion.1 = bf16[8,256,64]{1,2,0:T(8,128)(2,1)} fusion(bf16[8,256,64]{1,2,0:T(8,128)(2,1)S(1)} %copy-done.1, pred[8,256]{1,0:T(8,128)(4,1)S(1)} %get-tuple-element.27, pred[8,256]{1,0:T(8,128)(4,1)S(1)} %get-tuple-element.28, pred[8,256]{1,0:T(8,128)(4,1)S(1)} %get-tuple-element.29, pred[8,256]{1,0:T(8,128)(4,1)S(1)} %get-tuple-element.26, ...), kind=kLoop, calls=%fused_computation.4 | loop fusion | flops 524288 | bytes 536576 | tf_op jit(solution)/shard_map/jit(_where)/select_n | solution.py:379
  45.1 2.5 %select_select_fusion = bf16[8,256,256]{2,1,0:T(8,128)(2,1)} fusion(bf16[8,256,256]{2,1,0:T(8,128)(2,1)S(1)} %copy-done, pred[8,256]{1,0:T(8,128)(4,1)S(1)} %get-tuple-element.27, pred[8,256]{1,0:T(8,128)(4,1)S(1)} %get-tuple-element.28, pred[8,256]{1,0:T(8,128)(4,1)S(1)} %get-tuple-element.29, pred[8,256]{1,0:T(8,128)(4,1)S(1)} %get-tuple-element.26, ...), kind=kLoop, calls=%fused_computation | loop fusion | flops 2097152 | bytes 2121728 | tf_op jit(solution)/shard_map/jit(_where)/select_n | solution.py:378
  47.6 0.6 %copy.45 = bf16[4,8,512]{2,0,1:T(4,128)(2,1)} copy(bf16[4,8,512]{2,1,0:T(8,128)(2,1)S(1)} %bitcast.42) | data formatting | bytes 65536 | tf_op jit(solution)/shard_map/reshape | solution.py:381
  (40 shorter events, 0.8 us)
Async XLA Ops:
  0.6 4.1 %copy-start.4 = (bf16[256,4,128]{2,1,0:T(4,128)(2,1)S(1)}, bf16[256,4,128]{2,1,0:T(4,128)(2,1)}, u32[]{:S(2)}) copy-start(bf16[256,4,128]{2,1,0:T(4,128)(2,1)} %param.31) | copy-start | bytes 786436
  3.2 0.5 %copy-start.9 = (s32[8]{0:T(128)}, s32[8]{0:T(128)S(1)}, u32[]{:S(2)}) copy-start(s32[8]{0:T(128)S(1)} %add.27.valid_ref) | copy-start | bytes 100
  4.7 1.9 %copy-start.2 = (bf16[512,4,128]{2,1,0:T(4,128)(2,1)S(1)}, bf16[512,4,128]{2,1,0:T(4,128)(2,1)}, u32[]{:S(2)}) copy-start(bf16[512,4,128]{2,1,0:T(4,128)(2,1)} %param.28) | copy-start | bytes 1572868
  6.6 1.0 %copy-start.1 = (bf16[8,256,64]{1,2,0:T(8,128)(2,1)S(1)}, bf16[8,256,64]{1,2,0:T(8,128)(2,1)}, u32[]{:S(2)}) copy-start(bf16[8,256,64]{1,2,0:T(8,128)(2,1)} %param.22) | copy-start | bytes 786436
  7.5 1.0 %copy-start.3 = (bf16[512,4,64]{0,2,1:T(8,128)(2,1)S(1)}, bf16[512,4,64]{0,2,1:T(8,128)(2,1)}, u32[]{:S(2)}) copy-start(bf16[512,4,64]{0,2,1:T(8,128)(2,1)} %param.29) | copy-start | bytes 786436
  8.5 0.8 %copy-start.5 = (bf16[512,64]{0,1:T(8,128)(2,1)S(1)}, bf16[512,64]{0,1:T(8,128)(2,1)}, u32[]{:S(2)}) copy-start(bf16[512,64]{0,1:T(8,128)(2,1)} %param.26) | copy-start | bytes 196612
  9.4 0.8 %copy-start.6 = (bf16[8,4,512]{2,1,0:T(4,128)(2,1)S(1)}, bf16[8,4,512]{2,1,0:T(4,128)(2,1)}, u32[]{:S(2)}) copy-start(bf16[8,4,512]{2,1,0:T(4,128)(2,1)} %param.17) | copy-start | bytes 98308
  10.8 0.7 %copy-start.11 = (bf16[512]{0:T(512)(128)(2,1)S(1)}, bf16[512]{0:T(512)(128)(2,1)}, u32[]{:S(2)}) copy-start(bf16[512]{0:T(512)(128)(2,1)} %param.23) | copy-start | bytes 3076
  11.5 0.7 %copy-start.12 = (bf16[512]{0:T(512)(128)(2,1)S(1)}, bf16[512]{0:T(512)(128)(2,1)}, u32[]{:S(2)}) copy-start(bf16[512]{0:T(512)(128)(2,1)} %param.27) | copy-start | bytes 3076
  12.1 0.7 %copy-start.13 = (bf16[512]{0:T(512)(128)(2,1)S(1)}, bf16[512]{0:T(512)(128)(2,1)}, u32[]{:S(2)}) copy-start(bf16[512]{0:T(512)(128)(2,1)} %param.33) | copy-start | bytes 3076
  13.4 31.7 %copy-start = (bf16[8,256,256]{2,1,0:T(8,128)(2,1)S(1)}, bf16[8,256,256]{2,1,0:T(8,128)(2,1)}, u32[]{:S(2)}) copy-start(bf16[8,256,256]{2,1,0:T(8,128)(2,1)} %lat_hbm.1) | copy-start | bytes 3145732
  43.4 0.6 %copy-start.10 = (s32[8]{0:T(128)S(1)}, s32[8]{0:T(128)}, u32[]{:S(2)}) copy-start(s32[8]{0:T(128)} %copy-done.9) | copy-start | bytes 100
  44.1 1.0 %copy-start.8 = (bf16[32,256]{1,0:T(8,128)(2,1)S(1)}, bf16[32,256]{1,0:T(8,128)(2,1)}, u32[]{:S(2)}) copy-start(bf16[32,256]{1,0:T(8,128)(2,1)} %get-tuple-element.7) | copy-start | bytes 49156
  45.1 2.5 %copy-start.7 = (bf16[32,512]{1,0:T(8,128)(2,1)S(1)}, bf16[32,512]{1,0:T(8,128)(2,1)}, u32[]{:S(2)}) copy-start(bf16[32,512]{1,0:T(8,128)(2,1)} %get-tuple-element.6) | copy-start | bytes 98308

commit v2 on v1

--- a/solution.py
+++ b/solution.py
@@ -2,6 +2,7 @@
 
 import jax
 import jax.numpy as jnp
+import numpy as np
 from jax import lax
 from jax.experimental import pallas as pl
 from jax.experimental.pallas import tpu as pltpu
@@ -14,6 +15,7 @@
 F32 = jnp.float32
 BF16 = jnp.bfloat16
 NT = (((1,), (1,)), ((), ()))
+TN = (((0,), (0,)), ((), ()))
 
 
 def dot(a, b):
@@ -42,12 +44,13 @@
 
 def kernel(
     nk, nt, seqs, props, heads, qr, kvr, rope, vd, nope, model,
-    valid_ref, tokens_ref, g_pre_ref, g_q_ref, g_out_ref, table_ref, mask_ref,
+    prev_ref, accepted_ref, parents_ref, tokens_ref, g_pre_ref, g_q_ref, g_out_ref,
     wdq_hbm, wdkv_hbm, wkr_hbm, wuq_hbm, wqr_hbm, wuk_hbm, wuv_hbm, wout_hbm, lat_hbm, rot_hbm,
-    mixed_ref, latnew_ref, keynew_ref,
-    wdq, wdkv, wkr, wuq, wqr, wuk, wuv, wout, lat, rot,
+    mixed_ref, latout_hbm, rotout_hbm,
+    wdq, wdkv, wkr, wuq_raw, wqr, wuk_raw, wuv_raw, wout, lat, rot,
+    wuq, wuk, wuv, spread, table_ref, lat_out, rot_out,
     tok, buf1, buf2, buf3, lse3, buf4, buf5, qa, cs,
-    load_sem, send1, recv1, send2, recv2, send3, recv3, send3b, recv3b, send4, recv4, send5, recv5,
+    load_sem, store_sem, send1, recv1, send2, recv2, send3, recv3, send3b, recv3b, send4, recv4, send5, recv5,
 ):
     me_k = lax.axis_index("kv")
     me_t = lax.axis_index("tp")
@@ -66,8 +69,9 @@
     loads = []
     for i, (src, dst) in enumerate(
         (
-            (wdq_hbm, wdq), (wdkv_hbm, wdkv), (wkr_hbm, wkr), (wuq_hbm, wuq), (wqr_hbm, wqr),
-            (wuk_hbm, wuk), (lat_hbm, lat), (rot_hbm, rot), (wuv_hbm, wuv), (wout_hbm, wout),
+            (wdq_hbm, wdq), (wdkv_hbm, wdkv), (wkr_hbm, wkr), (wuq_hbm, wuq_raw), (wqr_hbm, wqr),
+            (wuk_hbm, wuk_raw), (lat_hbm, lat), (rot_hbm, rot), (wuv_hbm, wuv_raw),
+            (wout_hbm, wout),
         )
     ):
         copy = pltpu.make_async_copy(src, dst, load_sem.at[i])
@@ -91,20 +95,77 @@
 
     sent = []
 
-    tok[...] = tokens_ref[...].astype(F32)
-    x = tok[pl.ds(pl.multiple_of(me_t * group, group), group), :]
-    scaled = (x * g_pre_ref[...].astype(F32)).astype(BF16)
+    width = tokens_ref.shape[2]
+    for s in range(seqs):
+        own = tokens_ref[s].astype(F32)
+        for c in range(tok.shape[0]):
+            piece = own[:, c * LANES : min((c + 1) * LANES, width)]
+            if piece.shape[1] < LANES:
+                fill = jnp.zeros((props, LANES - piece.shape[1]), F32)
+                piece = jnp.concatenate([piece, fill], axis=1)
+            tok[c, pl.ds(s, props, stride=seqs), :] = piece
+    mine = pl.ds(pl.multiple_of(me_t * group, group), group)
+    x = jnp.concatenate([tok[c, mine, :] for c in range(tok.shape[0])], axis=1)[:, 0:width]
+    scaled = (x * g_pre_ref[...].astype(F32).reshape(1, width)).astype(BF16)
     squares = jnp.sum(x * x, axis=1, keepdims=True)
     for i in range(3):
         loads[i].wait()
     buf1[me_k, :, 0:qr] = dot(scaled, wdq[...])
     buf1[me_k, :, qr : qr + kvr] = dot(scaled, wdkv[...])
     buf1[me_k, :, qr + kvr : qr + kvr + LANES] = jnp.concatenate(
-        [dot(scaled, wkr[...]), jnp.broadcast_to(squares, (group, LANES - rope))], axis=1
+        [dot_nt(scaled, wkr[...]), jnp.broadcast_to(squares, (group, LANES - rope))], axis=1
     )
     pl.semaphore_wait(barrier, nk - 1 + nt - 1)
     copies = exchange(buf1, "kv", me_k, nk, send1, recv1)
     sent += copies
+
+    valid = [prev_ref[s] + accepted_ref[s] for s in range(seqs)]
+    sublane = lax.broadcasted_iota(jnp.int32, (seqs, LANES), 0)
+    lane = lax.broadcasted_iota(jnp.int32, (seqs, LANES), 1)
+    place = [jnp.zeros((seqs, LANES), jnp.int32) for j in range(props)]
+    kin = [jnp.zeros((seqs, LANES), jnp.int32) for j in range(props)]
+    for s in range(seqs):
+        depth, line = [], []
+        for j in range(props):
+            parent = parents_ref[j, s]
+            deep, bits = jnp.int32(0), jnp.int32(1 << j)
+            for m in range(j):
+                deep = jnp.where(parent == m, depth[m] + 1, deep)
+                bits = jnp.where(parent == m, line[m] + (1 << j), bits)
+            depth.append(deep)
+            line.append(bits)
+            place[j] = jnp.where(sublane == s, valid[s] + deep, place[j])
+            kin[j] = jnp.where(sublane == s, bits, kin[j])
+    half = rope // 2
+    frequency = jnp.zeros((1, LANES), F32)
+    for i in range(half):
+        value = float(np.float32(ROPE_BASE ** (-i / half)))
+        frequency = jnp.where(lax.rem(lane[0:1], half) == i, value, frequency)
+    angles = jnp.concatenate(place, axis=0).astype(F32) * frequency
+    table_ref[:, 0:LANES] = jnp.cos(angles)
+    table_ref[:, LANES:] = jnp.sin(angles)
+    own_seq = lax.rem(lane, seqs) == sublane
+    their = lax.div(lane, seqs)
+    linked = jnp.concatenate(
+        [
+            (own_seq & ((lax.shift_right_logical(bits, their) & 1) == 1)).astype(F32)
+            for bits in kin
+        ],
+        axis=0,
+    )[:, 0:tokens]
+    for i, raw, flat, size in (
+        (3, wuq_raw, wuq, nope), (5, wuk_raw, wuk, nope), (8, wuv_raw, wuv, vd)
+    ):
+        loads[i].wait()
+        count = raw.shape[0]
+        depth_rows = count // heads
+        spread[0:count, :] = raw[...].astype(F32)
+        for h in range(heads):
+            flat[:, h * size : (h + 1) * size] = spread[
+                pl.ds(h, depth_rows, stride=heads), :
+            ].astype(BF16)
+    for i in (4, 6, 7):
+        loads[i].wait()
     for copy in copies:
         copy.wait_recv()
     total = buf1[0]
@@ -116,7 +177,7 @@
     q_norm = (
         q_latent
         * lax.rsqrt(jnp.mean(q_latent * q_latent, axis=1, keepdims=True) + EPS)
-        * g_q_ref[...].astype(F32)
+        * g_q_ref[...].astype(F32).reshape(1, qr)
     )
     kv_latent = total[:, qr : qr + kvr] * scale
     latent = kv_latent * lax.rsqrt(jnp.mean(kv_latent * kv_latent, axis=1, keepdims=True) + EPS)
@@ -127,8 +188,6 @@
     buf2[me_t, :, qr + kvr :] = key.astype(BF16)
     copies = exchange(buf2, "tp", me_t, nt, send2, recv2)
     sent += copies
-    for i in range(3, 8):
-        loads[i].wait()
     for copy in copies:
         copy.wait_recv()
 
@@ -136,11 +195,9 @@
     q_all = gathered[:, 0:qr].astype(BF16)
     lat_new = gathered[:, qr : qr + kvr].astype(BF16)
     key_new = gathered[:, qr + kvr : qr + kvr + rope].astype(BF16)
-    latnew_ref[...] = lat_new
-    keynew_ref[...] = key_new
 
     q_nope = dot(q_all, wuq[...]).astype(BF16)
-    q_raw = dot(q_all, wqr[...])
+    q_raw = dot_nt(q_all, wqr[...])
     copies_wide = heads * rope // LANES
     cosine = jnp.concatenate([table_ref[:, 0:LANES]] * copies_wide, axis=1)
     sine = jnp.concatenate([table_ref[:, LANES:]] * copies_wide, axis=1)
@@ -161,8 +218,8 @@
         pick = pl.ds(s, per_seq, stride=seqs)
         q_lat = jnp.concatenate([qa[c, pick, :] for c in range(lat_tiles)], axis=1).astype(BF16)
         q_pos = qa[lat_tiles, pick, :][:, 0:rope].astype(BF16)
-        scores = (dot_nt(q_lat, lat[s]) + dot_nt(q_pos, rot[s])) * inv_root
-        seen = column < valid_ref[s]
+        scores = (dot_nt(q_lat, lat[s]) + dot(q_pos, rot[s])) * inv_root
+        seen = column < valid[s]
         peak = jnp.max(jnp.where(seen, scores, NEG_INF), axis=1, keepdims=True)
         weights = jnp.where(seen, jnp.exp(scores - peak), 0.0)
         mass = jnp.sum(weights, axis=1, keepdims=True)
@@ -174,8 +231,6 @@
             cs[c, pick, :] = mean[:, c * LANES : (c + 1) * LANES]
         cs[lat_tiles, pick, :] = jnp.broadcast_to(lse, (per_seq, LANES))
 
-    loads[8].wait()
-
     def up_value(means, h):
         high = means.astype(BF16)
         low = (means - high.astype(F32)).astype(BF16)
@@ -194,7 +249,7 @@
     q_lat = jnp.concatenate([qa[c] for c in range(lat_tiles)], axis=1).astype(BF16)
     q_pos = qa[lat_tiles][:, 0:rope].astype(BF16)
     scores = (dot_nt(q_lat, lat_new) + dot_nt(q_pos, key_new)) * inv_root
-    linked = jnp.concatenate([mask_ref[...]] * heads, axis=0) > 0.5
+    linked = jnp.concatenate([linked] * heads, axis=0) > 0.5
     peak = jnp.max(jnp.where(linked, scores, NEG_INF), axis=1, keepdims=True)
     weights = jnp.where(linked, jnp.exp(scores - peak), 0.0)
     mass = jnp.sum(weights, axis=1, keepdims=True)
@@ -203,6 +258,24 @@
     tree_vals = jnp.concatenate(
         [up_value(means[h * tokens : (h + 1) * tokens], h) for h in range(heads)], axis=0
     )
+    row = lax.broadcasted_iota(jnp.int32, (tokens, span), 0)
+    where_to = lax.broadcasted_iota(jnp.int32, (tokens, span), 1) + offset
+    row_pos = lax.broadcasted_iota(jnp.int32, (span, kvr), 0) + offset
+    lane_pos = lax.broadcasted_iota(jnp.int32, (rope, span), 1) + offset
+    stores = []
+    for s in range(seqs):
+        hit = (where_to - lax.div(row, seqs) == valid[s]) & (lax.rem(row, seqs) == s)
+        hit = hit.astype(F32).astype(BF16)
+        put = lax.dot_general(hit, lat_new, TN, preferred_element_type=F32)
+        landed = (row_pos >= valid[s]) & (row_pos < valid[s] + props)
+        lat_out[s] = jnp.where(landed, put, lat[s].astype(F32)).astype(BF16)
+        put = lax.dot_general(key_new, hit, TN, preferred_element_type=F32)
+        landed = (lane_pos >= valid[s]) & (lane_pos < valid[s] + props)
+        rot_out[s] = jnp.where(landed, put, rot[s].astype(F32)).astype(BF16)
+    for i, (src, dst) in enumerate(((lat_out, latout_hbm), (rot_out, rotout_hbm))):
+        copy = pltpu.make_async_copy(src, dst, store_sem.at[i])
+        copy.start()
+        stores.append(copy)
     loads[9].wait()
     for copy in copies:
         copy.wait_recv()
@@ -231,7 +304,7 @@
     buf5[me_k] = column_to_row(jnp.sum(mixed_raw * mixed_raw, axis=1, keepdims=True))
     copies = exchange(buf5, "kv", me_k, nk, send5, recv5)
     sent += copies
-    scaled_out = mixed_raw * g_out_ref[...].astype(F32)
+    scaled_out = mixed_raw * g_out_ref[...].astype(F32).reshape(1, mixed_raw.shape[1])
     for copy in copies:
         copy.wait_recv()
     total_sq = buf5[0]
@@ -242,18 +315,8 @@
     mixed_ref[...] = (scaled_out * factor).astype(BF16)
     for copy in sent:
         copy.wait_send()
-
-
-def lineage(parents):
-    props = parents.shape[1]
-    index = jnp.arange(props, dtype=jnp.int32)
-    rows = []
-    for j in range(props):
-        row = jnp.broadcast_to(index == j, (parents.shape[0], props))
-        for m in range(j):
-            row = row | ((parents[:, j : j + 1] == m) & rows[m])
-        rows.append(row)
-    return jnp.stack(rows, axis=1)
+    for copy in stores:
+        copy.wait()
 
 
 def local(
@@ -289,49 +352,42 @@
     rows = heads * count
     wide = qr + kvr + LANES
 
-    valid_len = prev_len + accepted
-    family = lineage(parents)
-    depths = jnp.sum(family.astype(jnp.int32), axis=2) - 1
-    positions = (valid_len[:, None] + depths).T.reshape(count)
-    half = rope // 2
-    frequency = ROPE_BASE ** (-jnp.arange(half, dtype=F32) / half)
-    angles = positions.astype(F32)[:, None] * jnp.tile(frequency, LANES // half)
-    table = jnp.concatenate([jnp.cos(angles), jnp.sin(angles)], axis=1)
-    same = jnp.eye(seqs, dtype=F32)
-    mask = (family.astype(F32).transpose(1, 0, 2)[:, :, :, None] * same[None, :, None, :]).reshape(
-        count, count
-    )
-    rows_in = tokens.transpose(1, 0, 2).reshape(count, width)
-
     vmem = pl.BlockSpec(memory_space=pltpu.VMEM)
     anywhere = pl.BlockSpec(memory_space=pl.ANY)
     dma = pltpu.SemaphoreType.DMA
     weights = (
         w_down_q,
         w_down_kv,
-        w_key_rope,
-        w_up_q.reshape(qr, heads * nope),
-        w_q_rope.reshape(qr, heads * rope),
-        w_up_key.reshape(kvr, heads * nope),
-        w_up_value.reshape(kvr, heads * vd),
+        w_key_rope.T,
+        w_up_q.reshape(qr * heads, nope),
+        w_q_rope.transpose(1, 2, 0).reshape(heads * rope, qr),
+        w_up_key.reshape(kvr * heads, nope),
+        w_up_value.reshape(kvr * heads, vd),
         w_out,
         cache_latent,
-        cache_rope,
-    )
-    mixed, lat_new, key_new = pl.pallas_call(
+        cache_rope.transpose(0, 2, 1),
+    )
+    mixed, new_latent, new_rope = pl.pallas_call(
         functools.partial(
             kernel, nk, nt, seqs, props, heads, qr, kvr, rope, vd, nope, width * nk
         ),
         out_shape=(
             jax.ShapeDtypeStruct((count, width_out), BF16),
-            jax.ShapeDtypeStruct((count, kvr), BF16),
-            jax.ShapeDtypeStruct((count, rope), BF16),
+            jax.ShapeDtypeStruct(cache_latent.shape, BF16),
+            jax.ShapeDtypeStruct((seqs, rope, span), BF16),
         ),
-        in_specs=[pl.BlockSpec(memory_space=pltpu.SMEM)] + [vmem] * 6 + [anywhere] * 10,
-        out_specs=(vmem, vmem, vmem),
+        in_specs=[pl.BlockSpec(memory_space=pltpu.SMEM)] * 3 + [vmem] * 4 + [anywhere] * 10,
+        out_specs=(vmem, anywhere, anywhere),
         scratch_shapes=[pltpu.VMEM(w.shape, BF16) for w in weights]
         + [
-            pltpu.VMEM((count, width), F32),
+            pltpu.VMEM((qr, heads * nope), BF16),
+            pltpu.VMEM((kvr, heads * nope), BF16),
+            pltpu.VMEM((kvr, heads * vd), BF16),
+            pltpu.VMEM((max(qr, kvr) * heads, LANES), F32),
+            pltpu.VMEM((count, 2 * LANES), F32),
+            pltpu.VMEM(cache_latent.shape, BF16),
+            pltpu.VMEM((seqs, rope, span), BF16),
+            pltpu.VMEM((pl.cdiv(width, LANES), count, LANES), F32),
             pltpu.VMEM((nk, group, wide), F32),
             pltpu.VMEM((nt, group, wide), BF16),
             pltpu.VMEM((nk, rows, vd), BF16),
@@ -341,6 +397,7 @@
             pltpu.VMEM((kvr // LANES + 1, rows, LANES), F32),
             pltpu.VMEM((kvr // LANES + 1, rows, LANES), F32),
             dma((10,)),
+            dma((2,)),
             dma((nk - 1,)),
             dma((nk - 1,)),
             dma((nt - 1,)),
@@ -356,31 +413,20 @@
         ],
         compiler_params=pltpu.CompilerParams(collective_id=0, has_side_effects=True),
     )(
-        valid_len,
-        rows_in,
-        g_pre.reshape(1, width),
-        g_q.reshape(1, qr),
-        g_out.reshape(1, width_out),
-        table,
-        mask,
+        prev_len,
+        accepted,
+        parents.T,
+        tokens,
+        g_pre,
+        g_q,
+        g_out,
         *weights,
     )
 
-    slot = (
-        lax.axis_index("kv") * span
-        + jnp.arange(span, dtype=jnp.int32)[None, :]
-        - valid_len[:, None]
-    )[:, :, None]
-    new_latent = cache_latent
-    new_rope = cache_rope
-    for j in range(props):
-        here = slot == j
-        new_latent = jnp.where(here, lat_new[j * seqs : (j + 1) * seqs, None, :], new_latent)
-        new_rope = jnp.where(here, key_new[j * seqs : (j + 1) * seqs, None, :], new_rope)
     return (
         mixed.reshape(props, seqs, width_out).transpose(1, 0, 2),
         new_latent,
-        new_rope,
+        new_rope.transpose(0, 2, 1),
     )
 
 

time: 48.6 us -> 34.5 us (0.71)
  local copies, waits for them, and re-layouts: 12.2 us -> 4.4 us
  other arithmetic: 6.06 us -> 0 us
    reshape x5 -> x0, local copies, waits for them, and re-layouts: 4.47 us -> none  [the longest x1 1.86 us: local(): w_up_value.reshape(kvr, heads * vd)]
    select_n x2 -> x0, other arithmetic: 3.51 us -> none  [the longest x1 2.47 us: local(): jnp.where(here, lat_new[j * seqs:(j + 1) * seqs, None, :], new_latent)]
    unnamed x31 -> x4, local copies, waits for them, and re-layouts: 4.75 us -> 3.01 us
    eq x4 -> x0, other arithmetic: 0.89 us -> none  [the longest x1 0.8 us: lineage(): row = row | (parents[:, j:j + 1] == m) & rows[m]]
    mul x2 -> x0, local copies, waits for them, and re-layouts: 0.78 us -> none  [the longest x1 0.69 us: local(): family.astype(F32).transpose(1, 0, 2)[:, :, :, None]]
    reshape x1, local copies, waits for them, and re-layouts: 0.63 us -> 1.39 us  [local(): mixed.reshape(props, seqs, width_out).transpose(1, 0, 2)]
    transpose x2 -> x0, local copies, waits for them, and re-layouts: 0.73 us -> none  [the longest x1 0.62 us: local(): rows_in = tokens.transpose(1, 0, 2).reshape(count, width)]
    slice x2 -> x0, local copies, waits for them, and re-layouts: 0.7 us -> none  [the longest x1 0.7 us: local(): key_new[j * seqs:(j + 1) * seqs, None, :]]
where the time goes in v2:
time: 34.5 us; the launch traced here: 34.2 us
  Pallas kernels  29.2 us (85%)
  local copies, waits for them, and re-layouts  4.4 us (13%)
  between operations  0.65 us (2%)
    pallas_call x1, Pallas kernels, local(): pl.pallas_call(functools.partial(kernel, nk, nt, seqs, props, heads, qr,...  29.2 us
    unnamed x4, local copies, waits for them, and re-layouts  3.01 us
    reshape x1, local copies, waits for them, and re-layouts, local(): mixed.reshape(props, seqs, width_out).transpose(1, 0, 2)  1.39 us

profile of v2, /device:TPU:0, one launch (start us, length us, event | category | flops | bytes accessed | tf_op | source)
XLA Modules:
  0.0 34.2 jit_solution(9201162319387100978)
XLA Ops:
  0.6 29.2 %shard_map.184 = (bf16[32,512]{1,0:T(8,128)(2,1)}, bf16[8,256,256]{2,1,0:T(8,128)(2,1)}, bf16[8,64,256]{2,1,0:T(8,128)(2,1)}) custom-call(s32[8]{0:T(128)} %prev_ref.1, s32[8]{0:T(128)} %accepted_ref.1, s32[4,8]{1,0:T(4,128)} %bitcast.23, bf16[8,4,512]{2,1,0:T(4,128)(2,1)} %tokens_ref.1, bf16[512]{0:T(512)(128)(2,1)} %g_pre_ref.1, bf16[512]{0:T(512)(128)(2,1)} %g_q_ref.1, ...), custom_call_target="tpu_custom_call" | custom-call | tf_op jit(solution)/shard_map/pallas_call | solution.py:370
  29.8 1.4 %copy.22 = bf16[4,8,512]{2,0,1:T(4,128)(2,1)} copy(bf16[4,8,512]{2,1,0:T(8,128)(2,1)} %bitcast.22) | data formatting | bytes 65536 | tf_op jit(solution)/shard_map/reshape | solution.py:427
  31.2 0.0 copy-start
  31.2 2.3 %copy.25 = bf16[8,256,256]{2,1,0:T(8,128)(2,1)} copy(bf16[8,256,256]{2,1,0:T(8,128)(2,1)} %get-tuple-element.13) | data formatting | bytes 2097152
  33.5 0.0 copy-done
  33.5 0.7 %copy.26 = bf16[8,256,64]{1,2,0:T(8,128)(2,1)} copy(bf16[8,256,64]{1,2,0:T(8,128)(2,1)S(1)} %bitcast.19) | data formatting | bytes 524288
Async XLA Ops:
  31.2 2.3 %copy-start = (bf16[8,64,256]{2,1,0:T(8,128)(2,1)S(1)}, bf16[8,64,256]{2,1,0:T(8,128)(2,1)}, u32[]{:S(2)}) copy-start(bf16[8,64,256]{2,1,0:T(8,128)(2,1)} %get-tuple-element.8) | copy-start | bytes 786436
